TPU v7x, 32 devices: a whole 2x2x4 slice. The times are simulated.
32 devices in a mesh: grp: 2 (over x), ep: 4 (over z), tp: 4 (over y, core).
Axes of the slice: x: 2, y: 2, z: 4, core: 2. Of those that a mesh axis runs over, the one named last changes fastest.
Arguments:
- token_rows: bfloat16 [4096, 2048], P(('grp', 'ep', 'tp')), parts along dimension 0, may hold values from -6 to 6
- norm_gain: float32 [2048], replicated, may hold values from 0.1 to 1.9
- norm_bias: float32 [2048], replicated, may hold values from -3 to 3
- expert_ids: int32 [4096, 2], P(('grp', 'ep', 'tp')), parts along dimension 0, may hold values from 0 to 3, as said below
- route_gates: float32 [4096, 2], P(('grp', 'ep', 'tp')), parts along dimension 0, may hold values from 0.1 to 1
- gate_weight: bfloat16 [4, 2048, 512], P('tp'), may hold values from -0.125 to 0.125
- up_weight: bfloat16 [4, 2048, 512], P('tp'), may hold values from -0.125 to 0.125
- down_weight: bfloat16 [4, 512, 2048], P('tp'), may hold values from -0.25 to 0.25
Outputs:
- combined: bfloat16 [4096, 2048], P(('grp', 'ep', 'tp')), parts along dimension 0
There are 2 independent parts, one for each index of `grp`. A program takes and returns all parts, laid end to end along the dimension named above; an argument that names none is the same for every part. Nothing has to cross between parts.
Inputs may be any that keep to these rules, and one draw needn't show every extreme that they name: `expert_ids`: the two experts of a token are different and lie in one group: both are among 4 * g to 4 * g + 3 for some g. In the rows of one device (aligned blocks of 128 rows) no expert is named more than 64 times, and in every such block each expert of one group is named exactly 64 times; that group is the same for all blocks of a draw.
All inputs are finite; a program needn't handle non-finite values.
Results may differ from a plain program's by a relative error of at most 0.01.
Values may be sent and summed in bfloat16 or wider, within the bound.
A program may use at most 64 MiB of HBM per device.

v0:
```python
import functools

import jax
import jax.numpy as jnp
from jax import lax
from jax.experimental import pallas as pl
from jax.experimental.pallas import tpu as pltpu
from jax.sharding import PartitionSpec as P

EPSILON = 1e-05
F32 = jnp.float32
BF16 = jnp.bfloat16
MESH = pl.DeviceIdType.MESH
CHUNK_ROWS = 32
NORM_ROWS = 16
BLOCKS = 1
VMEM_BYTES = 48 * 1024 * 1024
IN_SPACE = pltpu.HBM


def dot(a, b):
    return jnp.dot(a, b, preferred_element_type=F32)


def kernel(
    tp_count, cores, capacity, chunks,
    tokens_hbm, gain_hbm, bias_hbm, ids_hbm, gates_hbm, wg_hbm, wu_hbm, wd_hbm,
    out_ref,
    tokens, gain_ref, bias_ref, ids_ref, gates_ref, wg, wu, wd, normed,
    near_out, near_in, near_res, near_back, far_out, far_in, far_res, far_back, total,
    w_sem, near_send, near_recv, near_rsend, near_rrecv, far_send, far_recv, far_rsend, far_rrecv,
):
    tok_count, width = tokens.shape
    chips = tp_count // cores
    far = tp_count - cores
    rows = capacity // chunks
    block = width // BLOCKS
    me = lax.axis_index("tp")
    my_chip, my_core = me // cores, me % cores

    def peer(slot):
        return (my_chip + slot // cores) % chips * cores + (my_core + slot % cores) % cores

    def origin(slot):
        return (my_chip + chips - slot // cores) % chips * cores + (my_core + cores - slot % cores) % cores

    barrier = pltpu.get_barrier_semaphore()
    for slot in range(1, tp_count):
        pl.semaphore_signal(barrier, inc=1, device_id={"tp": peer(slot)}, device_id_type=MESH)
    pairs = (
        (ids_hbm, ids_ref), (tokens_hbm, tokens), (gates_hbm, gates_ref), (gain_hbm, gain_ref), (bias_hbm, bias_ref),
        (wg_hbm.at[0], wg), (wu_hbm.at[0], wu), (wd_hbm.at[0], wd),
    )
    loads = [pltpu.make_async_copy(src, dst, w_sem.at[i]) for i, (src, dst) in enumerate(pairs)]
    for load in loads:
        load.start()

    lanes = 128 * pl.cdiv(tp_count, 128)
    t_row = lax.broadcasted_iota(jnp.int32, (tok_count, tok_count), 0)
    t_col = lax.broadcasted_iota(jnp.int32, (tok_count, tok_count), 1)
    before = jnp.where(t_row < t_col, 1.0, 0.0).astype(BF16)
    expert_of_row = lax.broadcasted_iota(jnp.int32, (lanes, tok_count), 0)
    loads[0].wait()
    ids = ids_ref[...]
    first = ids[0:1, :] == expert_of_row
    second = ids[1:2, :] == expert_of_row
    named = jnp.where(first | second, 1.0, 0.0)
    rank = dot(named.astype(BF16), before)
    place_t = jnp.where(named > 0.5, rank, -1.0)

    def place_row(slot):
        return jnp.sum(jnp.where(expert_of_row == peer(slot), place_t, 0.0), axis=0, keepdims=True).astype(jnp.int32)

    def pick(slot, start, count):
        want = start + lax.broadcasted_iota(jnp.int32, (count, tok_count), 0)
        return jnp.where(place_row(slot) == want, 1.0, 0.0).astype(BF16)

    def far_copy(c, f):
        return pltpu.make_async_remote_copy(
            far_out.at[c, f], far_in.at[c, f], far_send.at[c, f], far_recv.at[c, f],
            device_id={"tp": peer(cores + f)}, device_id_type=MESH)

    def far_return(c, f, j):
        at = pl.ds(j * block, block)
        return pltpu.make_async_remote_copy(
            far_res.at[c, f, :, at], far_back.at[c, f, :, at], far_rsend.at[c, f, j], far_rrecv.at[c, f, j],
            device_id={"tp": origin(cores + f)}, device_id_type=MESH)

    def near_copy(s):
        return pltpu.make_async_remote_copy(
            near_out.at[s], near_in.at[s], near_send.at[s], near_recv.at[s],
            device_id={"tp": peer(s)}, device_id_type=MESH)

    def near_return(s):
        return pltpu.make_async_remote_copy(
            near_res.at[s], near_back.at[s], near_rsend.at[s], near_rrecv.at[s],
            device_id={"tp": origin(s)}, device_id_type=MESH)

    for c in range(chunks):
        picks = jnp.concatenate([pick(cores + f, c * rows, rows) for f in range(far)], axis=0)
        if c == 0:
            loads[1].wait()
        far_out[c] = dot(picks, tokens[...]).astype(BF16).reshape(far, rows, width)
        if c == 0:
            pl.semaphore_wait(barrier, tp_count - 1)
        for f in range(far):
            far_copy(c, f).start()
    near_picks = jnp.concatenate([pick(s, 0, capacity) for s in range(cores)], axis=0)
    packed = dot(near_picks, tokens[...]).astype(BF16).reshape(cores, capacity, width)
    near_in[0] = packed[0]
    for s in range(1, cores):
        near_out[s] = packed[s]
        near_copy(s).start()

    for load in loads[2:5]:
        load.wait()
    gates = gates_ref[...]
    place = place_t.T
    gate_of = (jnp.where(first, gates[0:1, :], 0.0) + jnp.where(second, gates[1:2, :], 0.0)).T
    lane = lax.broadcasted_iota(jnp.int32, (tok_count, lanes), 1)

    def norm(load_rows, count):
        gain = gain_ref[...]
        bias = bias_ref[...]

        def norm_block(i, carry):
            at = pl.multiple_of(i * NORM_ROWS, NORM_ROWS)
            x = load_rows(at).astype(F32)
            center = jnp.mean(x, axis=-1, keepdims=True)
            centered = x - center
            variance = jnp.mean(centered * centered, axis=-1, keepdims=True)
            normed[pl.ds(at, NORM_ROWS), :] = (centered * lax.rsqrt(variance + EPSILON) * gain + bias).astype(BF16)
            return carry

        lax.fori_loop(0, count // NORM_ROWS, norm_block, 0)

    def hidden_of(count):
        rows_in = normed[pl.ds(0, count), :]
        gate_act = dot(rows_in, wg[...])
        up_act = dot(rows_in, wu[...])
        return (gate_act / (1.0 + jnp.exp(-gate_act)) * up_act).astype(BF16)

    for s in range(1, cores):
        near_copy(s).wait_recv()
    norm(lambda at: near_in[at // capacity, pl.ds(pl.multiple_of(at % capacity, NORM_ROWS), NORM_ROWS), :], cores * capacity)
    for load in loads[5:]:
        load.wait()
    results = dot(hidden_of(cores * capacity), wd[...]).astype(BF16).reshape(cores, capacity, width)
    near_back[0] = results[0]
    for s in range(1, cores):
        near_res[s] = results[s]
        near_return(s).start()

    def far_step(c, carry):
        for f in range(far):
            far_copy(c, f).wait_recv()
        norm(lambda at: far_in[c, at // rows, pl.ds(pl.multiple_of(at % rows, NORM_ROWS), NORM_ROWS), :], far * rows)
        hidden = hidden_of(far * rows)
        for j in range(BLOCKS):
            at = pl.ds(j * block, block)
            far_res[c, :, :, at] = dot(hidden, wd[:, at]).astype(BF16).reshape(far, rows, block)
            for f in range(far):
                far_return(c, f, j).start()
        return carry

    lax.fori_loop(0, chunks, far_step, 0)

    def spread(slots, start, count):
        want = lax.broadcasted_iota(jnp.int32, (tok_count, len(slots) * count), 1)
        high = jnp.zeros(want.shape, F32)
        for i, slot in enumerate(slots):
            mine = lane == peer(slot)
            at = jnp.sum(jnp.where(mine, place, 0.0), axis=1, keepdims=True).astype(jnp.int32) - start
            gate = jnp.sum(jnp.where(mine, gate_of, 0.0), axis=1, keepdims=True)
            at = jnp.where((at >= 0) & (at < count), at + i * count, -1)
            high = high + jnp.where(at == want, gate, 0.0)
        coarse = high.astype(BF16)
        return jnp.concatenate([coarse, (high - coarse.astype(F32)).astype(BF16)], axis=1)

    for s in range(1, cores):
        near_return(s).wait_recv()
    weights = spread(range(cores), 0, capacity)
    back = near_back[...].reshape(cores * capacity, width)
    total[...] = dot(weights, jnp.concatenate([back, back], axis=0))

    for c in range(chunks):
        weights = spread(range(cores, tp_count), c * rows, rows)
        for j in range(BLOCKS):
            at = pl.ds(j * block, block)
            for f in range(far):
                far_return(c, f, j).wait_recv()
            back = far_back[c, :, :, at].reshape(far * rows, block)
            part = total[:, at] + dot(weights, jnp.concatenate([back, back], axis=0))
            if c + 1 < chunks:
                total[:, at] = part
            else:
                out_ref[:, at] = part.astype(BF16)
    for s in range(1, cores):
        near_copy(s).wait_send()
        near_return(s).wait_send()

    def drain(c, carry):
        for f in range(far):
            far_copy(c, f).wait_send()
            for j in range(BLOCKS):
                far_return(c, f, j).wait_send()
        return carry

    lax.fori_loop(0, chunks, drain, 0)


def shards(token_rows, norm_gain, norm_bias, expert_ids, route_gates, gate_weight, up_weight, down_weight):
    tok_count, width = token_rows.shape
    hidden = gate_weight.shape[2]
    tp_count = lax.axis_size("tp")
    capacity = min(4 * tok_count // tp_count, tok_count // 2)
    cores = 2
    far = tp_count - cores
    chunks = max(1, capacity // CHUNK_ROWS)
    rows = capacity // chunks
    near = pltpu.VMEM((cores, capacity, width), BF16)
    distant = pltpu.VMEM((chunks, far, rows, width), BF16)
    near_sem = pltpu.SemaphoreType.DMA((cores,))
    far_sem = pltpu.SemaphoreType.DMA((chunks, far))
    ret_sem = pltpu.SemaphoreType.DMA((chunks, far, BLOCKS))
    return pl.pallas_call(
        functools.partial(kernel, tp_count, cores, capacity, chunks),
        out_shape=pltpu.VMEM((tok_count, width), BF16),
        in_specs=[pl.BlockSpec(memory_space=IN_SPACE)] * 8,
        out_specs=pl.BlockSpec(memory_space=pltpu.VMEM),
        scratch_shapes=[
            pltpu.VMEM((tok_count, width), BF16),
            pltpu.VMEM((1, width), F32),
            pltpu.VMEM((1, width), F32),
            pltpu.VMEM((2, tok_count), jnp.int32),
            pltpu.VMEM((2, tok_count), F32),
            pltpu.VMEM((width, hidden), BF16),
            pltpu.VMEM((width, hidden), BF16),
            pltpu.VMEM((hidden, width), BF16),
            pltpu.VMEM((max(cores * capacity, far * rows), width), BF16),
            near, near, near, near,
            distant, distant, distant, distant,
            pltpu.VMEM((tok_count, width), F32),
            pltpu.SemaphoreType.DMA((8,)),
            near_sem, near_sem, near_sem, near_sem,
            far_sem, far_sem, ret_sem, ret_sem,
        ],
        compiler_params=pltpu.CompilerParams(
            collective_id=0, has_side_effects=True, vmem_limit_bytes=VMEM_BYTES
        ),
    )(
        *(pltpu.with_memory_space_constraint(x, pltpu.HBM) for x in (
            token_rows, norm_gain.reshape(1, width), norm_bias.reshape(1, width),
            expert_ids.T, route_gates.T, gate_weight, up_weight, down_weight,
        ))
    )


def solution(mesh):
    rows = P(("grp", "ep", "tp"), None)
    weight = P("tp", None, None)
    return jax.shard_map(
        shards, mesh=mesh,
        in_specs=(rows, P(), P(), rows, rows, weight, weight, weight),
        out_specs=rows, check_vma=False,
    )
```

profile of v0, /device:TPU:0, one launch (start us, length us, event | category | flops | bytes accessed | tf_op | source)
XLA Modules:
  0.0 28.0 jit_solution(16260328686249244330)
XLA Ops:
  0.0 27.2 %shard_map.82 = bf16[128,2048]{1,0:T(8,128)(2,1)S(1)} custom-call(bf16[128,2048]{1,0:T(8,128)(2,1)} %tokens_hbm.1, f32[1,2048]{1,0:T(1,128)} %bitcast.4, f32[1,2048]{1,0:T(1,128)} %bitcast.5, s32[2,128]{1,0:T(2,128)} %bitcast.6, f32[2,128]{1,0:T(2,128)} %bitcast.7, bf16[1,2048,512]{2,1,0:T(8,128)(2,1)} %wg_hbm.1, bf16[1,2048,512]{2,1,0:T(8,128)(2,1)} %wu_hbm.1, ...), custom_call_target="tpu_custom_call" | custom-call | tf_op jit(solution)/shard_map/pallas_call | solution.py:226
  27.2 0.8 %copy.10 = bf16[128,2048]{1,0:T(8,128)(2,1)} copy(bf16[128,2048]{1,0:T(8,128)(2,1)S(1)} %shard_map.82) | data formatting | bytes 1048576
where the time goes:
time: 28.3 us; the launch traced here: 28 us
  Pallas kernels  27.2 us (96%)
  local copies, waits for them, and re-layouts  0.8 us (3%)
    pallas_call x1, Pallas kernels, shards(): pl.pallas_call(functools.partial(kernel, tp_count, cores, capacity, chunk...  27.2 us
    unnamed x1, local copies, waits for them, and re-layouts  0.8 us

commit v1 on v0

--- a/solution.py
+++ b/solution.py
@@ -16,6 +16,9 @@
 BLOCKS = 1
 VMEM_BYTES = 48 * 1024 * 1024
 IN_SPACE = pltpu.HBM
+KEEP = 8
+STEP_ROWS = 32
+OUT_COLS = 512
 
 
 def dot(a, b):
@@ -209,12 +212,346 @@
     lax.fori_loop(0, chunks, drain, 0)
 
 
+def pair_kernel(tp_count, cores, start, sizes, opening, shared, *refs):
+    refs = list(refs)
+    ins = [refs.pop(0) for _ in range(8)]
+    base_ref = None if opening else refs.pop(0)
+    out_ref = refs.pop(0)
+    flag_ref = refs.pop(0) if shared else None
+    (tokens, scales, ids_all, gates_all, w_in, wd, both, total, near_back, far_out, raw, pool,
+     mine, mix_out, mix_in, far_res, far_back, sem, step_recv, pass_recv, back_recv, meta_recv) = refs[:22]
+    near_res, near_recv = refs[22:24] if opening else (None, None)
+    flag_out, flag_in, flag_recv, here = refs[24:] if shared else [None] * 4
+    tok_count, width = tokens.shape
+    steps, cap = len(sizes), sum(sizes)
+    starts = [sum(sizes[:k]) for k in range(steps)]
+    me = lax.axis_index("tp")
+    my_chip, my_core = me // cores, me % cores
+    partner = my_chip * cores + (my_core + 1) % cores
+    far = (my_chip + 1) % 2 * cores + my_core
+    cross = (my_chip + 1) % 2 * cores + (my_core + 1) % cores
+    peers = (me, partner, far, cross)
+    groups, group = 1, 0
+    if shared:
+        outer, inner = lax.axis_size("ep"), lax.axis_size("grp")
+        groups = outer * inner
+        group = lax.axis_index("ep") * inner + lax.axis_index("grp")
+
+    def member(k):
+        other = (group + k) % groups
+        return other, {"ep": other // inner, "grp": other % inner}
+
+    barrier = pltpu.get_barrier_semaphore()
+    for slot in range(1, tp_count):
+        pl.semaphore_signal(barrier, inc=1, device_id={"tp": peers[slot]}, device_id_type=MESH)
+    for k in range(1, groups):
+        other, where = member(k)
+
+        @pl.when(other > group)
+        def _(where=where):
+            pl.semaphore_signal(barrier, inc=1, device_id=where, device_id_type=MESH)
+
+    moves = [
+        (ins[3], ids_all.at[0], 0), (ins[0], tokens, 1), (ins[4], gates_all.at[0], 2),
+        (ins[1], scales.at[0], 3), (ins[2], scales.at[1], 3),
+        (ins[5].at[0], w_in.at[0], 4), (ins[6].at[0], w_in.at[1], 4), (ins[7].at[0], wd, 5),
+    ]
+    for src, dst, i in moves:
+        pltpu.make_async_copy(src, dst, sem.at[i]).start()
+
+    def landed(ref, i):
+        pltpu.make_async_copy(ref, ref, sem.at[i]).wait()
+
+    def copy(src, dst, send, recv, tp):
+        return pltpu.make_async_remote_copy(src, dst, sem.at[send], recv, device_id={"tp": tp}, device_id_type=MESH)
+
+    def span(k):
+        return pl.ds(starts[k], sizes[k])
+
+    def far_copy(k):
+        dst = raw if k == 0 and opening else pool.at[pl.ds(2 * starts[k], sizes[k])]
+        return copy(far_out.at[span(k)], dst, 0, step_recv.at[k], far)
+
+    def relay(k):
+        src = pool.at[pl.ds(2 * starts[k], sizes[k])]
+        return copy(src, pool.at[pl.ds(2 * starts[k] + sizes[k], sizes[k])], 4, pass_recv.at[0, k % 2], partner)
+
+    def mix(k):
+        return copy(mix_out.at[span(k)], mix_in.at[span(k)], 5, pass_recv.at[1, k % 2], partner)
+
+    def far_return(k):
+        return copy(far_res.at[span(k)], far_back.at[span(k)], 6, back_recv.at[(k + 1) // steps], far)
+
+    def meta(i, slot):
+        table = (ids_all, gates_all)[i]
+        return copy(table.at[0], table.at[slot], 1 + i, meta_recv.at[i], peers[slot])
+
+    def near_copy():
+        return copy(both.at[pl.ds(0, tok_count)], both.at[pl.ds(tok_count, tok_count)], 3, near_recv.at[0], partner)
+
+    def near_return():
+        return copy(near_res, near_back, 3, near_recv.at[1], partner)
+
+    def flag_copy(k):
+        return pltpu.make_async_remote_copy(
+            flag_out, flag_in.at[k], sem.at[7], flag_recv.at[0], device_id=member(k)[1], device_id_type=MESH)
+
+    def sent(ref, i):
+        pltpu.make_async_remote_copy(ref, ref, sem.at[i], sem.at[i], device_id={"tp": far}, device_id_type=MESH).wait_send()
+
+    def received(ref, recv):
+        pltpu.make_async_remote_copy(ref, ref, sem.at[0], recv, device_id={"tp": far}, device_id_type=MESH).wait_recv()
+
+    row = lax.broadcasted_iota(jnp.int32, (tok_count, tok_count), 0)
+    col = lax.broadcasted_iota(jnp.int32, (tok_count, tok_count), 1)
+    before = jnp.where(row < col, 1.0, 0.0).astype(BF16)
+
+    def leaves(slot):
+        low = peers[slot] // cores * cores
+        ids = ids_all[slot]
+        away = (ids < low) | (ids >= low + cores)
+        return jnp.where(away[0:1, :] | away[1:2, :], 1.0, 0.0)
+
+    def place_of(leaving):
+        rank = dot(jnp.broadcast_to(leaving, (16, tok_count)).astype(BF16), before)[0:1, :]
+        return jnp.where(leaving > 0.5, rank, -1.0)
+
+    def pick(place, k):
+        want = start + starts[k] + lax.broadcasted_iota(jnp.int32, (sizes[k], tok_count), 0)
+        return place.astype(jnp.int32) == want
+
+    def gate_row(slot):
+        mine_of = jnp.where(ids_all[slot] == me, gates_all[slot], 0.0)
+        return mine_of[0:1, :] + mine_of[1:2, :]
+
+    def column(chosen, values):
+        return jnp.sum(jnp.where(chosen, values, 0.0), axis=1, keepdims=True)
+
+    def pack(k, rows):
+        chosen = jnp.where(pick(place, k), 1.0, 0.0).astype(BF16)
+        far_out[span(k), :] = dot(chosen, rows).astype(BF16)
+
+    def norm(src, dst, count):
+        gain, bias = scales[0], scales[1]
+
+        def norm_block(i, carry):
+            at = pl.ds(pl.multiple_of(i * NORM_ROWS, NORM_ROWS), NORM_ROWS)
+            x = src[at, :].astype(F32)
+            center = jnp.mean(x, axis=-1, keepdims=True)
+            centered = x - center
+            variance = jnp.mean(centered * centered, axis=-1, keepdims=True)
+            dst[at, :] = (centered * lax.rsqrt(variance + EPSILON) * gain + bias).astype(BF16)
+            return carry
+
+        lax.fori_loop(0, count // NORM_ROWS, norm_block, 0)
+
+    def hidden_of(rows_in):
+        gate_act = dot(rows_in, w_in[0])
+        up_act = dot(rows_in, w_in[1])
+        return (gate_act / (1.0 + jnp.exp(-gate_act)) * up_act).astype(BF16)
+
+    blocks = [pl.ds(i, min(OUT_COLS, width - i)) for i in range(0, width, OUT_COLS)]
+    own_rows = both.at[pl.ds(0, tok_count)]
+
+    landed(ids_all.at[0], 0)
+    leaving = leaves(0)
+    place = place_of(leaving)
+    landed(tokens, 1)
+    if opening:
+        pack(0, tokens[...])
+    else:
+        landed(scales, 3)
+        norm(tokens, own_rows, tok_count)
+        pack(0, own_rows[...])
+    landed(gates_all.at[0], 2)
+    pl.semaphore_wait(barrier, tp_count - 1 + group)
+    for slot in range(tp_count - 1, 0, -1):
+        for i in range(2):
+            meta(i, slot).start()
+    far_copy(0).start()
+    for k in range(1, groups):
+        other, where = member(k)
+
+        @pl.when(other < group)
+        def _(where=where):
+            pl.semaphore_signal(here, inc=1, device_id=where, device_id_type=MESH)
+
+    if opening:
+        landed(scales, 3)
+        norm(tokens, own_rows, tok_count)
+    for k in range(1, steps):
+        pack(k, own_rows[...])
+        far_copy(k).start()
+    if opening:
+        near_copy().start()
+
+    for i in range(2):
+        received((ids_all, gates_all)[i].at[pl.ds(1, tp_count - 1)], meta_recv.at[i])
+    far_leaving, cross_leaving = leaves(2), leaves(3)
+    far_place, far_gate = place_of(far_leaving), gate_row(2)
+    cross_place, cross_gate = place_of(cross_leaving), gate_row(3)
+    if shared:
+        count = jnp.sum(leaving, axis=1, keepdims=True)
+        for other in (leaves(1), far_leaving, cross_leaving):
+            count = jnp.maximum(count, jnp.sum(other, axis=1, keepdims=True))
+        flag_out[...] = jnp.broadcast_to(jnp.where(count > cap, 1.0, 0.0), flag_out.shape)
+    landed(w_in, 4)
+    landed(wd, 5)
+    if opening:
+        gate_own = column(row == col, gate_row(0))
+        gate_near = column(row == col, gate_row(1))
+        near_copy().wait_recv()
+        hidden = hidden_of(both[...])
+        for cols in blocks:
+            result = dot(hidden, wd[:, cols])
+            total[:, cols] = result[:tok_count] * gate_own
+            near_res[:, cols] = (result[tok_count:] * gate_near).astype(BF16)
+        near_return().start()
+
+    far_copy(0).wait_recv()
+    if opening:
+        norm(raw, pool, sizes[0])
+    relay(0).start()
+    for k in range(steps):
+        gate_far = column(pick(far_place, k), far_gate)
+        gate_cross = column(pick(cross_place, k), cross_gate)
+        relay(k).wait_recv()
+        hidden = hidden_of(pool[pl.ds(2 * starts[k], 2 * sizes[k]), :])
+        for cols in blocks:
+            result = dot(hidden, wd[:, cols])
+            mine[pl.ds(0, sizes[k]), cols] = result[:sizes[k]] * gate_far
+            mix_out[span(k), cols] = (result[sizes[k]:] * gate_cross).astype(BF16)
+        mix(k).start()
+        if k + 1 < steps:
+            far_copy(k + 1).wait_recv()
+            relay(k + 1).start()
+        mix(k).wait_recv()
+        far_res[span(k), :] = (mine[pl.ds(0, sizes[k]), :] + mix_in[span(k), :].astype(F32)).astype(BF16)
+        far_return(k).start()
+        if shared and k == 0:
+            @pl.when(group < groups - 1)
+            def _():
+                pl.semaphore_wait(here, groups - 1 - group)
+
+            for other in range(1, groups):
+                flag_copy(other).start()
+
+    place_col = column(row == col, place).astype(jnp.int32)
+
+    def spread(at, count):
+        want = start + at + lax.broadcasted_iota(jnp.int32, (tok_count, count), 1)
+        return dot(jnp.where(place_col == want, 1.0, 0.0).astype(BF16), far_back[pl.ds(at, count), :])
+
+    if opening:
+        near_return().wait_recv()
+        total[...] = total[...] + near_back[...].astype(F32)
+    else:
+        total[...] = base_ref[...].astype(F32)
+    if shared:
+        received(flag_in.at[pl.ds(1, groups - 1)], flag_recv.at[0])
+        flag = flag_out[...]
+        for k in range(1, groups):
+            flag = jnp.maximum(flag, flag_in[k])
+        flag_ref[0, 0] = jnp.max(flag).astype(jnp.int32)
+    if steps > 1:
+        received(far_back.at[pl.ds(0, starts[-1])], back_recv.at[0])
+        total[...] = total[...] + spread(0, starts[-1])
+    far_return(steps - 1).wait_recv()
+    out_ref[...] = (total[...] + spread(starts[-1], sizes[-1])).astype(BF16)
+
+    for i in (0, 4, 5, 6):
+        sent(far_out, i)
+    for i in range(2):
+        sent((ids_all, gates_all)[i].at[pl.ds(1, tp_count - 1)], 1 + i)
+    if opening:
+        sent(both, 3)
+    if shared:
+        sent(flag_in.at[pl.ds(1, groups - 1)], 7)
+
+
+def pair_call(tp_count, cores, start, sizes, shared, arrays, base=None):
+    tok_count, width = arrays[0].shape
+    hidden = arrays[5].shape[2]
+    opening = base is None
+    cap = sum(sizes)
+    groups = lax.axis_size("ep") * lax.axis_size("grp")
+    whole = pltpu.VMEM((tok_count, width), BF16)
+    part = pltpu.VMEM((cap, width), BF16)
+    dma = pltpu.SemaphoreType.DMA
+    scratch = [
+        whole,
+        pltpu.VMEM((2, 1, width), F32),
+        pltpu.VMEM((tp_count, 2, tok_count), jnp.int32),
+        pltpu.VMEM((tp_count, 2, tok_count), F32),
+        pltpu.VMEM((2, width, hidden), BF16),
+        pltpu.VMEM((hidden, width), BF16),
+        pltpu.VMEM((2 * tok_count, width), BF16),
+        pltpu.VMEM((tok_count, width), F32),
+        whole,
+        part,
+        pltpu.VMEM((sizes[0], width), BF16),
+        pltpu.VMEM((2 * cap, width), BF16),
+        pltpu.VMEM((max(sizes), width), F32),
+        part, part, part, part,
+        dma((8,)), dma((len(sizes),)), dma((2, 2)), dma((2,)), dma((2,)),
+    ]
+    if opening:
+        scratch += [whole, dma((2,))]
+    if shared:
+        scratch += [
+            pltpu.VMEM((8, 128), F32), pltpu.VMEM((groups, 8, 128), F32), dma((1,)), pltpu.SemaphoreType.REGULAR,
+        ]
+    out_shape = [pltpu.VMEM((tok_count, width), BF16)]
+    out_specs = [pl.BlockSpec(memory_space=pltpu.VMEM)]
+    if shared:
+        out_shape.append(pltpu.SMEM((1, 1), jnp.int32))
+        out_specs.append(pl.BlockSpec(memory_space=pltpu.SMEM))
+    in_specs = [pl.BlockSpec(memory_space=IN_SPACE)] * len(arrays)
+    arrays = [pltpu.with_memory_space_constraint(x, pltpu.HBM) for x in arrays]
+    if not opening:
+        arrays.append(base)
+        in_specs.append(pl.BlockSpec(memory_space=pltpu.VMEM))
+    return pl.pallas_call(
+        functools.partial(pair_kernel, tp_count, cores, start, sizes, opening, shared),
+        out_shape=out_shape,
+        in_specs=in_specs,
+        out_specs=out_specs,
+        scratch_shapes=scratch,
+        compiler_params=pltpu.CompilerParams(
+            collective_id=0 if opening else 1, has_side_effects=True, vmem_limit_bytes=VMEM_BYTES
+        ),
+    )(*arrays)
+
+
+def cut(rows):
+    return [min(STEP_ROWS, rows - at) for at in range(0, rows, STEP_ROWS)]
+
+
+def pair_shards(tp_count, cores, arrays):
+    tok_count = arrays[0].shape[0]
+    cap = tok_count - (tok_count // KEEP if KEEP else 0)
+    if cap == tok_count:
+        return pair_call(tp_count, cores, 0, cut(cap), False, arrays)[0]
+    out, flag = pair_call(tp_count, cores, 0, cut(cap), True, arrays)
+    return lax.cond(
+        flag[0, 0] > 0,
+        lambda: pair_call(tp_count, cores, cap, cut(tok_count - cap), False, arrays, out)[0],
+        lambda: out,
+    )
+
+
 def shards(token_rows, norm_gain, norm_bias, expert_ids, route_gates, gate_weight, up_weight, down_weight):
     tok_count, width = token_rows.shape
     hidden = gate_weight.shape[2]
     tp_count = lax.axis_size("tp")
     capacity = min(4 * tok_count // tp_count, tok_count // 2)
     cores = 2
+    arrays = [
+        token_rows, norm_gain.reshape(1, width), norm_bias.reshape(1, width),
+        expert_ids.T, route_gates.T, gate_weight, up_weight, down_weight,
+    ]
+    if tp_count == 2 * cores:
+        return pair_shards(tp_count, cores, arrays)
     far = tp_count - cores
     chunks = max(1, capacity // CHUNK_ROWS)
     rows = capacity // chunks
@@ -248,12 +585,7 @@
         compiler_params=pltpu.CompilerParams(
             collective_id=0, has_side_effects=True, vmem_limit_bytes=VMEM_BYTES
         ),
-    )(
-        *(pltpu.with_memory_space_constraint(x, pltpu.HBM) for x in (
-            token_rows, norm_gain.reshape(1, width), norm_bias.reshape(1, width),
-            expert_ids.T, route_gates.T, gate_weight, up_weight, down_weight,
-        ))
-    )
+    )(*(pltpu.with_memory_space_constraint(x, pltpu.HBM) for x in arrays))
 
 
 def solution(mesh):

time: 28.3 us -> 26.8 us (0.947)
  Pallas kernels: 27.2 us -> 25.9 us
    pallas_call x1, Pallas kernels: 27.2 us -> 25.9 us  [pair_call(): pl.pallas_call(functools.partial(pair_kernel, tp_count, cores, start, siz...]
where the time goes in v1:
time: 26.8 us; the launch traced here: 26.7 us
  Pallas kernels  25.9 us (97%)
  local copies, waits for them, and re-layouts  0.8 us (3%)
    pallas_call x1, Pallas kernels, pair_call(): pl.pallas_call(functools.partial(pair_kernel, tp_count, cores, start, siz...  25.9 us
    unnamed x1, local copies, waits for them, and re-layouts  0.8 us

profile of v1, /device:TPU:0, one launch (start us, length us, event | category | flops | bytes accessed | tf_op | source)
XLA Modules:
  0.0 26.7 jit_solution(16576535154639738210)
XLA Ops:
  0.0 25.9 %shard_map.84 = (bf16[128,2048]{1,0:T(8,128)(2,1)S(1)}, s32[1,1]{1,0:T(1,128)S(4)}) custom-call(bf16[128,2048]{1,0:T(8,128)(2,1)} %refs_0_.1, f32[1,2048]{1,0:T(1,128)} %bitcast.5, f32[1,2048]{1,0:T(1,128)} %bitcast.7, s32[2,128]{1,0:T(2,128)} %bitcast.9, f32[2,128]{1,0:T(2,128)} %bitcast.11, bf16[1,2048,512]{2,1,0:T(8,128)(2,1)} %refs_5_.1, ...), custom_call_target="tpu_custom_call" | custom-call | tf_op jit(solution)/shard_map/pallas_call | solution.py:514
  25.9 0.8 %copy.15 = bf16[128,2048]{1,0:T(8,128)(2,1)} copy(bf16[128,2048]{1,0:T(8,128)(2,1)S(1)} %get-tuple-element.40) | data formatting | bytes 1048576
  (1 shorter events, 0.0 us)

commit v2 on v1

--- a/solution.py
+++ b/solution.py
@@ -19,6 +19,7 @@
 KEEP = 8
 STEP_ROWS = 32
 OUT_COLS = 512
+TAIL_COLS = 1024
 
 
 def dot(a, b):
@@ -256,8 +257,11 @@
         (ins[1], scales.at[0], 3), (ins[2], scales.at[1], 3),
         (ins[5].at[0], w_in.at[0], 4), (ins[6].at[0], w_in.at[1], 4), (ins[7].at[0], wd, 5),
     ]
-    for src, dst, i in moves:
-        pltpu.make_async_copy(src, dst, sem.at[i]).start()
+    def load(some):
+        for src, dst, i in some:
+            pltpu.make_async_copy(src, dst, sem.at[i]).start()
+
+    load(moves[:5])
 
     def landed(ref, i):
         pltpu.make_async_copy(ref, ref, sem.at[i]).wait()
@@ -279,8 +283,11 @@
     def mix(k):
         return copy(mix_out.at[span(k)], mix_in.at[span(k)], 5, pass_recv.at[1, k % 2], partner)
 
-    def far_return(k):
-        return copy(far_res.at[span(k)], far_back.at[span(k)], 6, back_recv.at[(k + 1) // steps], far)
+    def far_return(k, part=None):
+        if part is None:
+            return copy(far_res.at[span(k)], far_back.at[span(k)], 6, back_recv.at[0], far)
+        at = (span(k), halves[part])
+        return copy(far_res.at[at], far_back.at[at], 6, back_recv.at[1 + part], far)
 
     def meta(i, slot):
         table = (ids_all, gates_all)[i]
@@ -351,12 +358,14 @@
         return (gate_act / (1.0 + jnp.exp(-gate_act)) * up_act).astype(BF16)
 
     blocks = [pl.ds(i, min(OUT_COLS, width - i)) for i in range(0, width, OUT_COLS)]
+    halves = [pl.ds(i, min(TAIL_COLS, width - i)) for i in range(0, width, TAIL_COLS)]
     own_rows = both.at[pl.ds(0, tok_count)]
 
     landed(ids_all.at[0], 0)
     leaving = leaves(0)
     place = place_of(leaving)
     landed(tokens, 1)
+    load(moves[5:])
     if opening:
         pack(0, tokens[...])
     else:
@@ -397,17 +406,6 @@
         flag_out[...] = jnp.broadcast_to(jnp.where(count > cap, 1.0, 0.0), flag_out.shape)
     landed(w_in, 4)
     landed(wd, 5)
-    if opening:
-        gate_own = column(row == col, gate_row(0))
-        gate_near = column(row == col, gate_row(1))
-        near_copy().wait_recv()
-        hidden = hidden_of(both[...])
-        for cols in blocks:
-            result = dot(hidden, wd[:, cols])
-            total[:, cols] = result[:tok_count] * gate_own
-            near_res[:, cols] = (result[tok_count:] * gate_near).astype(BF16)
-        near_return().start()
-
     far_copy(0).wait_recv()
     if opening:
         norm(raw, pool, sizes[0])
@@ -427,7 +425,11 @@
             relay(k + 1).start()
         mix(k).wait_recv()
         far_res[span(k), :] = (mine[pl.ds(0, sizes[k]), :] + mix_in[span(k), :].astype(F32)).astype(BF16)
-        far_return(k).start()
+        if k + 1 < steps:
+            far_return(k).start()
+        else:
+            for part in range(len(halves)):
+                far_return(k, part).start()
         if shared and k == 0:
             @pl.when(group < groups - 1)
             def _():
@@ -436,11 +438,22 @@
             for other in range(1, groups):
                 flag_copy(other).start()
 
+    if opening:
+        gate_own = column(row == col, gate_row(0))
+        gate_near = column(row == col, gate_row(1))
+        near_copy().wait_recv()
+        hidden = hidden_of(both[...])
+        for cols in blocks:
+            result = dot(hidden, wd[:, cols])
+            total[:, cols] = result[:tok_count] * gate_own
+            near_res[:, cols] = (result[tok_count:] * gate_near).astype(BF16)
+        near_return().start()
+
     place_col = column(row == col, place).astype(jnp.int32)
 
     def spread(at, count):
         want = start + at + lax.broadcasted_iota(jnp.int32, (tok_count, count), 1)
-        return dot(jnp.where(place_col == want, 1.0, 0.0).astype(BF16), far_back[pl.ds(at, count), :])
+        return jnp.where(place_col == want, 1.0, 0.0).astype(BF16)
 
     if opening:
         near_return().wait_recv()
@@ -455,9 +468,11 @@
         flag_ref[0, 0] = jnp.max(flag).astype(jnp.int32)
     if steps > 1:
         received(far_back.at[pl.ds(0, starts[-1])], back_recv.at[0])
-        total[...] = total[...] + spread(0, starts[-1])
-    far_return(steps - 1).wait_recv()
-    out_ref[...] = (total[...] + spread(starts[-1], sizes[-1])).astype(BF16)
+        total[...] = total[...] + dot(spread(0, starts[-1]), far_back[pl.ds(0, starts[-1]), :])
+    last = spread(starts[-1], sizes[-1])
+    for part, cols in enumerate(halves):
+        far_return(steps - 1, part).wait_recv()
+        out_ref[:, cols] = (total[:, cols] + dot(last, far_back[span(steps - 1), cols])).astype(BF16)
 
     for i in (0, 4, 5, 6):
         sent(far_out, i)
@@ -493,7 +508,7 @@
         pltpu.VMEM((2 * cap, width), BF16),
         pltpu.VMEM((max(sizes), width), F32),
         part, part, part, part,
-        dma((8,)), dma((len(sizes),)), dma((2, 2)), dma((2,)), dma((2,)),
+        dma((8,)), dma((len(sizes),)), dma((2, 2)), dma((1 + pl.cdiv(width, TAIL_COLS),)), dma((2,)),
     ]
     if opening:
         scratch += [whole, dma((2,))]

time: 26.8 us -> 26.1 us (0.974)
  Pallas kernels: 25.9 us -> 25.1 us
    pallas_call x1, Pallas kernels: 25.9 us -> 25.1 us  [pair_call(): pl.pallas_call(functools.partial(pair_kernel, tp_count, cores, start, siz...]
where the time goes in v2:
time: 26.1 us; the launch traced here: 26 us
  Pallas kernels  25.1 us (96%)
  local copies, waits for them, and re-layouts  0.8 us (3%)
    pallas_call x1, Pallas kernels, pair_call(): pl.pallas_call(functools.partial(pair_kernel, tp_count, cores, start, siz...  25.1 us
    unnamed x1, local copies, waits for them, and re-layouts  0.8 us

profile of v2, /device:TPU:0, one launch (start us, length us, event | category | flops | bytes accessed | tf_op | source)
XLA Modules:
  0.0 26.0 jit_solution(7937204240798439828)
XLA Ops:
  0.0 25.1 %shard_map.84 = (bf16[128,2048]{1,0:T(8,128)(2,1)S(1)}, s32[1,1]{1,0:T(1,128)S(4)}) custom-call(bf16[128,2048]{1,0:T(8,128)(2,1)} %refs_0_.1, f32[1,2048]{1,0:T(1,128)} %bitcast.5, f32[1,2048]{1,0:T(1,128)} %bitcast.7, s32[2,128]{1,0:T(2,128)} %bitcast.9, f32[2,128]{1,0:T(2,128)} %bitcast.11, bf16[1,2048,512]{2,1,0:T(8,128)(2,1)} %refs_5_.1, ...), custom_call_target="tpu_custom_call" | custom-call | tf_op jit(solution)/shard_map/pallas_call | solution.py:529
  25.2 0.8 %copy.15 = bf16[128,2048]{1,0:T(8,128)(2,1)} copy(bf16[128,2048]{1,0:T(8,128)(2,1)S(1)} %get-tuple-element.40) | data formatting | bytes 1048576
  (1 shorter events, 0.0 us)
